TPU v7x, 32 devices: a whole 2x2x4 slice. The times are simulated.
32 devices in a mesh: rep: 2 (over x), fs: 4 (over z), tp: 4 (over y, core).
Axes of the slice: x: 2, y: 2, z: 4, core: 2. Of those that a mesh axis runs over, the one named last changes fastest.
Arguments:
- tokens: bfloat16 [6144, 2048], P(('rep', 'fs'), 'tp'), may hold values from -6 to 6
- gain_mix: bfloat16 [2048], replicated, may hold values from 0.099609375 to 1.8984375
- query_weight: bfloat16 [2048, 1024], P('fs', 'tp'), may hold values from -0.125 to 0.125
- key_weight: bfloat16 [2048, 1024], P('fs', 'tp'), may hold values from -0.125 to 0.125
- value_weight: bfloat16 [2048, 2048], P('fs', 'tp'), may hold values from -0.125 to 0.125
- gate_weight: bfloat16 [2048, 2048], P('fs', 'tp'), may hold values from -0.125 to 0.125
- decay_rate: float32 [8], P('tp'), may hold values from 0.0006510417 to 0.05
- out_weight: bfloat16 [2048, 2048], P('tp', 'fs'), may hold values from -0.125 to 0.125
- gain_mlp: bfloat16 [2048], replicated, may hold values from 0.099609375 to 1.8984375
- up_weight: bfloat16 [2048, 8192], P('fs', 'tp'), may hold values from -0.125 to 0.125
- down_weight: bfloat16 [8192, 2048], P('tp', 'fs'), may hold values from -0.0625 to 0.0625
Outputs:
- layer_out: bfloat16 [6144, 2048], P(('rep', 'fs'), 'tp')
All inputs are finite; a program needn't handle non-finite values.
Results may differ from a plain program's by a relative error of at most 0.019.
Values may be sent and summed in bfloat16 or wider, within the bound.
A program may use at most 128 MiB of HBM per device.

v0:
```python
import jax
import jax.numpy as jnp
from jax import lax
from jax.sharding import PartitionSpec as P

DK = 128
DV = 256
BLK = 128


epsilon = 1e-06
highest = lax.Precision.HIGHEST


def rms_rows(rows, gain):
    values = rows.astype(jnp.float32)
    scaled = values * lax.rsqrt(jnp.mean(values * values, axis=-1, keepdims=True) + epsilon)
    return (scaled * gain.astype(jnp.float32)).astype(jnp.bfloat16)


def retain(query, keys, values, rate, block):
    length, head_count, key_width = query.shape
    value_width = values.shape[-1]
    block_count = length // block
    log_decay = -rate
    positions = jnp.arange(block, dtype=jnp.float32)
    distance = positions[:, None] - positions[None, :]
    causal = distance >= 0
    inside = jnp.where(
        causal[None],
        jnp.exp(log_decay[:, None, None] * jnp.where(causal, distance, 0.0)[None]),
        0.0,
    )
    key_scale = jnp.exp(log_decay[None, :] * (block - 1.0 - positions)[:, None])
    query_scale = jnp.exp(log_decay[None, :] * (positions + 1.0)[:, None])
    carry_decay = jnp.exp(log_decay * block)
    query_blocks = query.reshape(block_count, block, head_count, key_width)
    key_blocks = keys.reshape(block_count, block, head_count, key_width) * key_width ** (-0.5)
    value_blocks = values.reshape(block_count, block, head_count, value_width)

    def advance(state, blocks):
        q_block, k_block, v_block = blocks
        scores = jnp.einsum("ihd,jhd->hij", q_block, k_block, precision=highest) * inside
        inner = jnp.einsum("hij,jhe->ihe", scores, v_block, precision=highest)
        cross = (
            jnp.einsum("ihd,hde->ihe", q_block, state, precision=highest) * query_scale[:, :, None]
        )
        update = jnp.einsum(
            "jhd,jhe->hde", k_block * key_scale[:, :, None], v_block, precision=highest
        )
        return (state * carry_decay[:, None, None] + update, inner + cross)

    initial = jnp.zeros((head_count, key_width, value_width), jnp.float32)
    _, results = lax.scan(advance, initial, (query_blocks, key_blocks, value_blocks))
    return results.reshape(length, head_count, value_width)


def gated_heads(retained, gate):
    length, head_count, value_width = retained.shape
    normed = retained * lax.rsqrt(jnp.mean(retained * retained, axis=-1, keepdims=True) + epsilon)
    gated = jax.nn.silu(gate.reshape(length, head_count, value_width)) * normed
    return gated.reshape(length, head_count * value_width).astype(jnp.bfloat16)


def add_rows(left, piece):
    return jnp.dot(left, piece, preferred_element_type=jnp.float32)


def local(
    tokens,
    gain_mix,
    query_weight,
    key_weight,
    value_weight,
    gate_weight,
    decay_rate,
    out_weight,
    gain_mlp,
    up_weight,
    down_weight,
):
    length = tokens.shape[0]
    whole_rows = lax.all_gather(tokens, "tp", axis=1, tiled=True)
    normed = rms_rows(whole_rows, gain_mix)

    def add_pair(pieces):
        return (add_rows(normed, pieces[0]), add_rows(normed, pieces[1]))

    query, keys = add_pair(
        (
            lax.all_gather(query_weight, "fs", axis=0, tiled=True),
            lax.all_gather(key_weight, "fs", axis=0, tiled=True),
        )
    )
    values, gate = add_pair(
        (
            lax.all_gather(value_weight, "fs", axis=0, tiled=True),
            lax.all_gather(gate_weight, "fs", axis=0, tiled=True),
        )
    )
    head_local = decay_rate.shape[0]
    retained = retain(
        query.reshape(length, head_local, DK),
        keys.reshape(length, head_local, DK),
        values.reshape(length, head_local, DV),
        decay_rate,
        BLK,
    )
    hidden = gated_heads(retained, gate)
    mix_terms = jnp.dot(
        hidden,
        lax.all_gather(out_weight, "fs", axis=1, tiled=True),
        preferred_element_type=jnp.float32,
    )
    mix_share = lax.psum_scatter(
        mix_terms.astype(jnp.bfloat16), "tp", scatter_dimension=1, tiled=True
    ).astype(jnp.float32)
    mixed = (tokens.astype(jnp.float32) + mix_share).astype(jnp.bfloat16)
    mixed_rows = lax.all_gather(mixed, "tp", axis=1, tiled=True)
    normed_mlp = rms_rows(mixed_rows, gain_mlp)
    upward = add_rows(normed_mlp, lax.all_gather(up_weight, "fs", axis=0, tiled=True))
    active = jnp.square(jax.nn.relu(upward)).astype(jnp.bfloat16)
    mlp_terms = jnp.dot(
        active,
        lax.all_gather(down_weight, "fs", axis=1, tiled=True),
        preferred_element_type=jnp.float32,
    )
    mlp_share = lax.psum_scatter(
        mlp_terms.astype(jnp.bfloat16), "tp", scatter_dimension=1, tiled=True
    ).astype(jnp.float32)
    return (mixed.astype(jnp.float32) + mlp_share).astype(jnp.bfloat16)


def solution(mesh):
    return jax.shard_map(
        local,
        mesh=mesh,
        in_specs=(
            P(("rep", "fs"), "tp"),
            P(),
            P("fs", "tp"),
            P("fs", "tp"),
            P("fs", "tp"),
            P("fs", "tp"),
            P("tp"),
            P("tp", "fs"),
            P(),
            P("fs", "tp"),
            P("tp", "fs"),
        ),
        out_specs=P(("rep", "fs"), "tp"),
        check_vma=False,
    )
```

profile of v0, /device:TPU:0, one launch (start us, length us, event | category | flops | bytes accessed | tf_op | source)
XLA Modules:
  0.0 679.4 jit_solution(13676328698701324082)
XLA Ops:
  12.0 28.2 %all-gather.10.cloned.1.call-done = bf16[768,2048]{1,0:T(8,128)(2,1)} async-done(((bf16[768,512]{1,0:T(8,128)(2,1)}), bf16[768,2048]{1,0:T(8,128)(2,1)}) %all-gather.10.cloned.1.call-update) | async-done | bytes 3145744 | tf_op jit(solution)/shard_map/all_gather | solution.py:83
  40.2 2.6 fusion.16
  42.7 44.7 %all-gather.16.cloned.1.call-done = bf16[2048,512]{1,0:T(8,128)(2,1)} async-done(((bf16[512,512]{1,0:T(8,128)(2,1)}), bf16[2048,512]{1,0:T(8,128)(2,1)}) %all-gather.16.cloned.1.call-update) | async-done | bytes 2097168 | tf_op jit(solution)/shard_map/all_gather | solution.py:97
  87.4 4.4 fusion.34
  91.8 2.2 reshape_reshape.7
  94.0 21.9 %all-gather.14.cloned.1.call-done = bf16[2048,256]{1,0:T(8,128)(2,1)} async-done(((bf16[512,256]{1,0:T(8,128)(2,1)}), bf16[2048,256]{1,0:T(8,128)(2,1)}) %all-gather.14.cloned.1.call-update) | async-done | bytes 1048592 | tf_op jit(solution)/shard_map/all_gather | solution.py:92
  115.8 3.2 convolution_multiply_fusion.1
  119.4 25.2 %all-gather.18.cloned.1.call-done = bf16[2048,256]{1,0:T(8,128)(2,1)} async-done(((bf16[512,256]{1,0:T(8,128)(2,1)}), bf16[2048,256]{1,0:T(8,128)(2,1)}) %all-gather.18.cloned.1.call-update) | async-done | bytes 1048592 | tf_op jit(solution)/shard_map/all_gather | solution.py:91
  144.6 3.2 fusion.32
  147.8 1.3 reshape_reshape.8
  149.1 24.6 %while.15 = (s32[]{:T(128)}, f32[2,128,256]{2,1,0:T(8,128)S(1)}, f32[6,128,2,256]{1,3,2,0:T(8,128)S(1)}, f32[2]{0:T(128)S(1)}, f32[6,128,2,128]{3,2,1,0:T(2,128)...) while((s32[]{:T(128)}, f32[2,128,256]{2,1,0:T(8,128)S(1)}, ...), condition=%wide.region_2.3_spmd.clone.clone.clone, body=%wide.region_1.2_spmd.clone.clone.clone.sunk | while | flops 352846336 | bytes 4019380 | solution.py:54
  173.7 2.1 copy.30
  178.6 12.5 %all-gather.12.cloned.1.call-done = bf16[2048,512]{1,0:T(8,128)(2,1)} async-done(((bf16[512,512]{1,0:T(8,128)(2,1)}), bf16[2048,512]{1,0:T(8,128)(2,1)}) %all-gather.12.cloned.1.call-update) | async-done | bytes 2097168 | tf_op jit(solution)/shard_map/all_gather | solution.py:98
  191.1 45.9 %all-gather.20.cloned.1.call-done = bf16[512,2048]{1,0:T(8,128)(2,1)} async-done(((bf16[512,512]{1,0:T(8,128)(2,1)}), bf16[512,2048]{1,0:T(8,128)(2,1)}) %all-gather.20.cloned.1.call-update) | async-done | bytes 2097168 | tf_op jit(solution)/shard_map/all_gather | solution.py:112
  237.0 8.9 %convolution_convert_fusion.1 = bf16[768,2048]{1,0:T(8,128)(2,1)} fusion(bf16[512,2048]{1,0:T(8,128)(2,1)} %all-gather.20.cloned.1.call-done, f32[768,512]{1,0:T(8,128)} %bitcast.68, f32[768,512]{1,0:T(8,128)S(1)} %bitcast.67, bf16[2048,512]{1,0:T(8,128)(2,1)} %all-gather.12.cloned.1.call-done, bf16[768,2048]{1,0:T(8,128)(2,1)} %all-gather.10.cloned.1.call-done, ...), kind=kOutput, calls=%fused_computation.37 | convolution fusion | flops 3231842304 | bytes 13642752 | tf_op jit(solution)/shard_map/dot_general | solution.py:110
  246.1 36.6 %reduce-scatter.3.cloned.1.call-done = bf16[768,512]{1,0:T(8,128)(2,1)} async-done(((bf16[768,2048]{1,0:T(8,128)(2,1)}), bf16[768,512]{1,0:T(8,128)(2,1)}) %reduce-scatter.3.cloned.1.call-update) | async-done | bytes 786448 | tf_op jit(solution)/shard_map/reduce_scatter | solution.py:115
  282.7 2.2 add_convert_fusion.1
  286.5 27.1 %all-gather.22.cloned.1.call-done = bf16[768,2048]{1,0:T(8,128)(2,1)} async-done(((bf16[768,512]{1,0:T(8,128)(2,1)}), bf16[768,2048]{1,0:T(8,128)(2,1)}) %all-gather.22.cloned.1.call-update) | async-done | bytes 3145744 | tf_op jit(solution)/shard_map/all_gather | solution.py:119
  313.6 2.7 fusion.19
  316.3 148.5 %all-gather.24.cloned.1.call-done = bf16[2048,2048]{1,0:T(8,128)(2,1)} async-done(((bf16[512,2048]{1,0:T(8,128)(2,1)}), bf16[2048,2048]{1,0:T(8,128)(2,1)}) %all-gather.24.cloned.1.call-update) | async-done | bytes 8388624 | tf_op jit(solution)/shard_map/all_gather | solution.py:121
  464.8 149.2 %all-gather.26.cloned.1.call-done = bf16[2048,2048]{1,0:T(8,128)(2,1)} async-done(((bf16[2048,512]{1,0:T(8,128)(2,1)}), bf16[2048,2048]{1,0:T(8,128)(2,1)}) %all-gather.26.cloned.1.call-update) | async-done | bytes 8388624 | tf_op jit(solution)/shard_map/all_gather | solution.py:125
  614.0 20.6 %convolution_convert_fusion = bf16[768,2048]{1,0:T(8,128)(2,1)} fusion(bf16[2048,2048]{1,0:T(8,128)(2,1)} %all-gather.26.cloned.1.call-done, bf16[2048,2048]{1,0:T(8,128)(2,1)} %all-gather.24.cloned.1.call-done, bf16[768,2048]{1,0:T(8,128)(2,1)S(1)} %copy-done.2, f32[2048]{0:T(1024)S(1)} %convert_element_type.58, f32[768]{0:T(1024)S(1)} %add_rsqrt_fusion), kind=kOutput, calls=%fused_computation.36 | convolution fusion | flops 12897484800 | bytes 23079936 | tf_op jit(solution)/shard_map/dot_general | solution.py:123
  634.6 36.1 %reduce-scatter.5.cloned.1.call-done = bf16[768,512]{1,0:T(8,128)(2,1)} async-done(((bf16[768,2048]{1,0:T(8,128)(2,1)}), bf16[768,512]{1,0:T(8,128)(2,1)}) %reduce-scatter.5.cloned.1.call-update) | async-done | bytes 786448 | tf_op jit(solution)/shard_map/reduce_scatter | solution.py:128
  670.7 2.2 add_convert_fusion
  (91 shorter events, 34.4 us)
Async XLA Ops:
  6.5 33.6 %all-gather.10.cloned.1.call-start = ((), (), s32[]{:S(2)}) async-start(), calls=%async_computation.2 | async-start | bytes 3932160 | tf_op jit(solution)/shard_map/all_gather | solution.py:83
  7.3 80.2 %all-gather.16.cloned.1.call-start = ((), (), s32[]{:S(2)}) async-start(), calls=%async_computation.5 | async-start | bytes 2621440 | tf_op jit(solution)/shard_map/all_gather | solution.py:97
  8.0 107.8 %all-gather.14.cloned.1.call-start = ((), (), s32[]{:S(2)}) async-start(), calls=%async_computation.4 | async-start | bytes 1310720 | tf_op jit(solution)/shard_map/all_gather | solution.py:92
  8.7 135.9 %all-gather.18.cloned.1.call-start = ((), (), s32[]{:S(2)}) async-start(), calls=%async_computation.6 | async-start | bytes 1310720 | tf_op jit(solution)/shard_map/all_gather | solution.py:91
  9.3 181.8 %all-gather.12.cloned.1.call-start = ((), (), s32[]{:S(2)}) async-start(), calls=%async_computation.3 | async-start | bytes 2621440 | tf_op jit(solution)/shard_map/all_gather | solution.py:98
  9.9 227.1 %all-gather.20.cloned.1.call-start = ((), (), s32[]{:S(2)}) async-start(), calls=%async_computation.7 | async-start | bytes 2621440 | tf_op jit(solution)/shard_map/all_gather | solution.py:112
  10.5 272.2 %reduce-scatter.3.cloned.1.call-start = ((), (), s32[]{:S(2)}) async-start(), calls=%async_computation.8 | async-start | bytes 3932160 | tf_op jit(solution)/shard_map/reduce_scatter | solution.py:115
  175.9 1.4 copy-start.1
  246.0 36.7 %copy-start.3 = (bf16[768,512]{1,0:T(8,128)(2,1)S(1)}, bf16[768,512]{1,0:T(8,128)(2,1)}, u32[]{:S(2)}) copy-start(bf16[768,512]{1,0:T(8,128)(2,1)} %param.13) | copy-start | bytes 2359300
  246.0 40.5 %copy-start.4 = (bf16[2048]{0:T(1024)(128)(2,1)S(1)}, bf16[2048]{0:T(1024)(128)(2,1)}, u32[]{:S(2)}) copy-start(bf16[2048]{0:T(1024)(128)(2,1)} %param.21) | copy-start | bytes 12292
  246.0 67.6 %all-gather.22.cloned.1.call-start = ((), (), s32[]{:S(2)}) async-start(), calls=%async_computation.9 | async-start | bytes 3932160 | tf_op jit(solution)/shard_map/all_gather | solution.py:119
  284.9 179.9 %all-gather.24.cloned.1.call-start = ((), (), s32[]{:S(2)}) async-start(), calls=%async_computation.10 | async-start | bytes 10485760 | tf_op jit(solution)/shard_map/all_gather | solution.py:121
  285.6 328.4 %all-gather.26.cloned.1.call-start = ((), (), s32[]{:S(2)}) async-start(), calls=%async_computation.11 | async-start | bytes 10485760 | tf_op jit(solution)/shard_map/all_gather | solution.py:125
  286.2 384.5 %reduce-scatter.5.cloned.1.call-start = ((), (), s32[]{:S(2)}) async-start(), calls=%async_computation.12 | async-start | bytes 3932160 | tf_op jit(solution)/shard_map/reduce_scatter | solution.py:128
  313.6 300.5 %copy-start.2 = (bf16[768,2048]{1,0:T(8,128)(2,1)S(1)}, bf16[768,2048]{1,0:T(8,128)(2,1)}, u32[]{:S(2)}) copy-start(bf16[768,2048]{1,0:T(8,128)(2,1)} %all-gather.22.cloned.1.call-done) | copy-start | bytes 9437188
  634.6 36.1 %copy-start = (bf16[768,512]{1,0:T(8,128)(2,1)S(1)}, bf16[768,512]{1,0:T(8,128)(2,1)}, u32[]{:S(2)}) copy-start(bf16[768,512]{1,0:T(8,128)(2,1)} %add_convert_fusion.1) | copy-start | bytes 2359300
Sparse Core Ops, SparseCore 0:
  8.9 31.2 all-gather.9
  41.7 45.6 all-gather.15
  89.0 26.7 all-gather.13
  117.2 27.3 all-gather.17
  146.0 45.0 all-gather.11
  192.5 44.4 all-gather.19
  246.1 36.5 reduce-scatter.2
  285.0 28.5 all-gather.21
  315.1 149.5 all-gather.23
  466.2 147.7 all-gather.25
  634.8 35.8 reduce-scatter.4
where the time goes:
time: 680 us; the launch traced here: 679 us
  waiting for transfers between devices  581 us (85%)
  matrix products  52.7 us (8%)
  local copies, waits for them, and re-layouts  20 us (3%)
  between operations  13.4 us (2%)
  other arithmetic  11.8 us (2%)
    all_gather x1, waiting for transfers between devices, local(): lax.all_gather(down_weight, 'fs', axis=1, tiled=True)  149 us
    all_gather x1, waiting for transfers between devices, local(): lax.all_gather(up_weight, 'fs', axis=0, tiled=True)  148 us
    all_gather x1, waiting for transfers between devices, local(): lax.all_gather(out_weight, 'fs', axis=1, tiled=True)  45.9 us
    all_gather x1, waiting for transfers between devices, local(): lax.all_gather(value_weight, 'fs', axis=0, tiled=True)  44.7 us
    reduce_scatter x1, waiting for transfers between devices, local(): lax.psum_scatter(mix_terms.astype(jnp.bfloat16), 'tp', scatter_dimension=...  36.6 us
    reduce_scatter x1, waiting for transfers between devices, local(): lax.psum_scatter(mlp_terms.astype(jnp.bfloat16), 'tp', scatter_dimension=...  36.1 us
    all_gather x1, waiting for transfers between devices, local(): whole_rows = lax.all_gather(tokens, 'tp', axis=1, tiled=True)  28.2 us
    all_gather x1, waiting for transfers between devices, local(): mixed_rows = lax.all_gather(mixed, 'tp', axis=1, tiled=True)  27.1 us
  transfers between devices with their start and end apart: 11, of which 11 were waited for; matrix products, arithmetic and copies ran while one was open for 7% of the time, Pallas kernels for 0%

commit v1 on v0

v1 whole, which is shorter than its diff:
```python
import jax
import jax.numpy as jnp
from jax import lax
from jax.sharding import PartitionSpec as P


DK = 128
DV = 256
EPS = 1e-06

ORDER = (2, 1, 3)


def rms_rows(rows, gain):
    values = rows.astype(jnp.float32)
    scaled = values * lax.rsqrt(jnp.mean(values * values, axis=-1, keepdims=True) + EPS)
    return (scaled * gain.astype(jnp.float32)).astype(jnp.bfloat16)


def shift(x, axis, n, by):
    return lax.ppermute(x, axis, [(k, (k + by) % n) for k in range(n)])


def far_pieces(chunk, n):
    if n != 4:
        return [shift(chunk, "fs", n, s) for s in range(1, n)]
    me = lax.axis_index("fs")
    two = lax.ppermute(chunk, "fs", [(0, 2), (1, 3), (2, 0), (3, 1)])
    left = lax.ppermute(chunk, "fs", [(0, 1), (1, 2), (2, 3)])
    right = lax.ppermute(chunk, "fs", [(1, 0), (2, 1), (3, 2)])
    ends = lax.ppermute(two, "fs", [(1, 0), (2, 3)])
    return [jnp.where(me == 0, ends, left), two, jnp.where(me == 3, ends, right)]


def gather(weight, dim, n, reps):
    width = weight.shape[dim]
    me = lax.axis_index("fs")
    starts = [lax.rem(me - s + n, n) * width for s in range(n)]
    if reps != 2:
        return list(zip([weight] + far_pieces(weight, n), starts))
    p = lax.axis_index("rep")
    half = width // 2
    mine = far_pieces(lax.dynamic_slice_in_dim(weight, p * half, half, axis=dim), n)
    pieces = [(weight, starts[0])]
    for s in ORDER if n == 4 else range(1, n):
        other = shift(mine[s - 1], "rep", 2, 1)
        pieces.append((mine[s - 1], starts[s] + p * half))
        pieces.append((other, starts[s] + (1 - p) * half))
    return pieces


def assemble(pieces, dim, width):
    shape = list(pieces[0][0].shape)
    shape[dim] = width
    out = jnp.zeros(shape, pieces[0][0].dtype)
    for piece, start in pieces:
        out = lax.dynamic_update_slice_in_dim(out, piece, start, axis=dim)
    return out


def product(left, right):
    return jnp.dot(left, right, preferred_element_type=jnp.float32)


def core_swap(x, n):
    return lax.ppermute(x, "tp", [(k, k ^ 1) for k in range(n)])


def gather_features(block, n):
    rows, width = block.shape
    me = lax.axis_index("tp")
    other = me + 1 - 2 * lax.rem(me, 2)
    out = jnp.zeros((rows, width * n), block.dtype)
    out = lax.dynamic_update_slice_in_dim(out, block, me * width, axis=1)
    out = lax.dynamic_update_slice_in_dim(out, core_swap(block, n), other * width, axis=1)
    for d in range(2, n, 2):
        far = shift(block, "tp", n, d)
        near = core_swap(far, n)
        out = lax.dynamic_update_slice_in_dim(out, far, lax.rem(me - d + n, n) * width, axis=1)
        out = lax.dynamic_update_slice_in_dim(out, near, lax.rem(other - d + n, n) * width, axis=1)
    return out


def scatter_sum(terms, n):
    width = terms.shape[1] // n
    me = lax.axis_index("tp")
    other = me + 1 - 2 * lax.rem(me, 2)
    total = None
    for d in list(range(2, n, 2)) + [0]:
        mine = lax.dynamic_slice_in_dim(terms, lax.rem(me + d, n) * width, width, axis=1)
        theirs = lax.dynamic_slice_in_dim(terms, lax.rem(other + d, n) * width, width, axis=1)
        pair = mine.astype(jnp.float32) + core_swap(theirs, n).astype(jnp.float32)
        if d:
            pair = shift(pair.astype(jnp.bfloat16), "tp", n, d).astype(jnp.float32)
        total = pair if total is None else total + pair
    return total


def retain(query, keys, values, rate):
    length, heads, _ = query.shape
    positions = jnp.arange(length, dtype=jnp.float32)
    distance = positions[:, None] - positions[None, :]
    causal = distance >= 0
    outs = []
    for h in range(heads):
        decay = jnp.where(causal, jnp.exp(-rate[h] * jnp.where(causal, distance, 0.0)), 0.0)
        scores = jnp.einsum(
            "id,jd->ij", query[:, h], keys[:, h], preferred_element_type=jnp.float32
        )
        scores = (scores * (DK ** -0.5) * decay).astype(jnp.bfloat16)
        outs.append(jnp.dot(scores, values[:, h], preferred_element_type=jnp.float32))
    return jnp.stack(outs, axis=1)


def gated_heads(retained, gate):
    length, heads, width = retained.shape
    normed = retained * lax.rsqrt(jnp.mean(retained * retained, axis=-1, keepdims=True) + EPS)
    gated = jax.nn.silu(gate.reshape(length, heads, width)) * normed
    return gated.reshape(length, heads * width).astype(jnp.bfloat16)


def solution(mesh):
    n_fs, n_tp, n_rep = mesh.shape["fs"], mesh.shape["tp"], mesh.shape["rep"]

    def layer(
        tokens, gain_mix, query_weight, key_weight, value_weight, gate_weight,
        decay_rate, out_weight, gain_mlp, up_weight, down_weight,
    ):
        length = tokens.shape[0]
        width = tokens.shape[1] * n_tp
        heads = decay_rate.shape[0]
        whole = gather_features(tokens, n_tp)
        first = jnp.concatenate([query_weight, key_weight, value_weight, gate_weight], axis=1)
        first_parts = gather(first, 0, n_fs, n_rep)
        out_parts = gather(out_weight, 1, n_fs, n_rep)
        up_parts = gather(up_weight, 0, n_fs, n_rep)
        down_parts = gather(down_weight, 1, n_fs, n_rep)

        normed = rms_rows(whole, gain_mix)
        qkvg = product(normed, assemble(first_parts, 0, width))
        a, b, c = heads * DK, 2 * heads * DK, 2 * heads * DK + heads * DV
        low = qkvg[:, :c].astype(jnp.bfloat16)
        retained = retain(
            low[:, :a].reshape(length, heads, DK),
            low[:, a:b].reshape(length, heads, DK),
            low[:, b:c].reshape(length, heads, DV),
            decay_rate,
        )
        hidden = gated_heads(retained, qkvg[:, c:])
        mix_terms = product(hidden, assemble(out_parts, 1, width)).astype(jnp.bfloat16)
        mixed = (tokens.astype(jnp.float32) + scatter_sum(mix_terms, n_tp)).astype(jnp.bfloat16)
        normed_mlp = rms_rows(gather_features(mixed, n_tp), gain_mlp)
        upward = product(normed_mlp, assemble(up_parts, 0, width))
        active = jnp.square(jax.nn.relu(upward)).astype(jnp.bfloat16)
        mlp_terms = product(active, assemble(down_parts, 1, width)).astype(jnp.bfloat16)
        return (mixed.astype(jnp.float32) + scatter_sum(mlp_terms, n_tp)).astype(jnp.bfloat16)

    return jax.shard_map(
        layer,
        mesh=mesh,
        in_specs=(
            P(("rep", "fs"), "tp"), P(), P("fs", "tp"), P("fs", "tp"), P("fs", "tp"),
            P("fs", "tp"), P("tp"), P("tp", "fs"), P(), P("fs", "tp"), P("tp", "fs"),
        ),
        out_specs=P(("rep", "fs"), "tp"),
        check_vma=False,
    )
```

time: 680 us -> 433 us (0.64); the launches traced: 679 us -> 425 us
  waiting for transfers between devices: 581 us -> 216 us
  starting transfers between devices: 0.61 us -> 90.6 us
  local copies, waits for them, and re-layouts: 20 us -> 60.5 us
  matrix products: 52.7 us -> 37.7 us
  between operations: 13.4 us -> 1.8 us
    all_gather x9 -> x0, waiting for transfers between devices: 503 us -> none  [the longest x1 149 us: local(): lax.all_gather(down_weight, 'fs', axis=1, tiled=True)]
    ppermute x0 -> x40, waiting for transfers between devices: none -> 216 us  [the longest x16 140 us: shift(): return lax.ppermute(x, axis, [(k, (k + by) % n) for k in range(n)])]
    ppermute x0 -> x40, starting transfers between devices: none -> 90.6 us  [the longest x4 51.9 us: far_pieces(): two = lax.ppermute(chunk, 'fs', [(0, 2), (1, 3), (2, 0), (3, 1)])]
    reduce_scatter x2 -> x0, waiting for transfers between devices: 72.7 us -> none  [the longest x1 36.6 us: local(): lax.psum_scatter(mix_terms.astype(jnp.bfloat16), 'tp', scatter_dimension=...]
    dynamic_update_slice x0 -> x27, local copies, waits for them, and re-layouts: none -> 29.6 us  [the longest x20 26.6 us: assemble(): out = lax.dynamic_update_slice_in_dim(out, piece, start, axis=dim)]
    dot_general x29 -> x5, matrix products: 52.7 us -> 37.7 us  [the longest x3 34.3 us: product(): return jnp.dot(left, right, preferred_element_type=jnp.float32)]
    dynamic_update_slice x0 -> x9, other arithmetic: none -> 14.7 us  [the longest x8 14.1 us: assemble(): out = lax.dynamic_update_slice_in_dim(out, piece, start, axis=dim)]
  transfers between devices with their start and end apart: 11 -> 40, of which waited for: 11 -> 20; matrix products, arithmetic and copies ran while one was open for 7% -> 21% of each run, Pallas kernels for 0% -> 0%
where the time goes in v1:
time: 433 us; the launch traced here: 425 us
  waiting for transfers between devices  216 us (50%)
  starting transfers between devices  90.6 us (21%)
  local copies, waits for them, and re-layouts  60.5 us (14%)
  matrix products  37.7 us (9%)
  other arithmetic  18.2 us (4%)
    ppermute x16, waiting for transfers between devices, shift(): return lax.ppermute(x, axis, [(k, (k + by) % n) for k in range(n)])  140 us
    ppermute x4, waiting for transfers between devices, far_pieces(): two = lax.ppermute(chunk, 'fs', [(0, 2), (1, 3), (2, 0), (3, 1)])  57 us
    ppermute x4, starting transfers between devices, far_pieces(): two = lax.ppermute(chunk, 'fs', [(0, 2), (1, 3), (2, 0), (3, 1)])  51.9 us
    dot_general x3, matrix products, product(): return jnp.dot(left, right, preferred_element_type=jnp.float32)  34.3 us
    dynamic_update_slice x20, local copies, waits for them, and re-layouts, assemble(): out = lax.dynamic_update_slice_in_dim(out, piece, start, axis=dim)  26.6 us
    ppermute x4, waiting for transfers between devices, far_pieces(): ends = lax.ppermute(two, 'fs', [(1, 0), (2, 3)])  17.8 us
    ppermute x16, starting transfers between devices, shift(): return lax.ppermute(x, axis, [(k, (k + by) % n) for k in range(n)])  15.5 us
    dynamic_update_slice x8, other arithmetic, assemble(): out = lax.dynamic_update_slice_in_dim(out, piece, start, axis=dim)  14.1 us
  transfers between devices with their start and end apart: 40, of which 20 were waited for; matrix products, arithmetic and copies ran while one was open for 21% of the time, Pallas kernels for 0%

profile of v1, /device:TPU:0, one launch (start us, length us, event | category | flops | bytes accessed | tf_op | source)
XLA Modules:
  0.0 425.2 jit_solution(11150639581587563002)
XLA Ops:
  7.2 3.5 collective-permute-start.13
  19.3 4.4 %broadcast.70.clone.1 = bf16[2048,2048]{1,0:T(8,128)(2,1)} broadcast(bf16[]{:T(256)} %constant.67.clone.1), dimensions={} | broadcast | bytes 8388610 | tf_op jit(solution)/shard_map/broadcast.7
  25.1 4.4 %broadcast.70.clone = bf16[2048,2048]{1,0:T(8,128)(2,1)} broadcast(bf16[]{:T(256)} %constant.67.clone.1), dimensions={} | broadcast | bytes 8388610 | tf_op jit(solution)/shard_map/broadcast.7
  42.5 3.9 collective-permute-start.3
  49.3 4.8 %collective-permute-done.14 = bf16[512,256]{1,0:T(8,128)(2,1)} collective-permute-done((bf16[512,256]{1,0:T(8,128)(2,1)S(1)}, bf16[512,256]{1,0:T(8,128)(2,1)}, u32[]{:S(2)}, u32[]{:S(2)}) %collective-permute-start.14) | collective-permute-done | bytes 262176 | tf_op jit(solution)/shard_map/ppermute | solution.py:21
  58.1 45.1 %collective-permute-start.30 = (bf16[2048,256]{1,0:T(8,128)(2,1)}, bf16[2048,256]{1,0:T(8,128)(2,1)}, u32[]{:S(2)}, u32[]{:S(2)}) collective-permute-start(bf16[2048,256]{1,0:T(8,128)(2,1)} %constant_dynamic-slice_fusion.2), channel_id=1, source_target_pairs={{0,8},{4,12},{8,0},{12,4},{1,9},{5,13},{9,1},{13,5},{2,10},{6,14},... | collective-permute-start | bytes 3145736 | tf_op jit(solution)/shard_map/ppermute | solution.py:28
  104.9 26.8 %collective-permute-done.3 = bf16[256,1536]{1,0:T(8,128)(2,1)} collective-permute-done((bf16[256,1536]{1,0:T(8,128)(2,1)}, bf16[256,1536]{1,0:T(8,128)(2,1)}, u32[]{:S(2)}, u32[]{:S(2)}) %collective-permute-start.3) | collective-permute-done | bytes 786464 | tf_op jit(solution)/shard_map/ppermute | solution.py:28
  142.9 11.4 %collective-permute-done.23 = bf16[256,2048]{1,0:T(8,128)(2,1)} collective-permute-done((bf16[256,2048]{1,0:T(8,128)(2,1)}, bf16[256,2048]{1,0:T(8,128)(2,1)}, u32[]{:S(2)}, u32[]{:S(2)}) %collective-permute-start.23) | collective-permute-done | bytes 1048608 | tf_op jit(solution)/shard_map/ppermute | solution.py:28
  157.9 18.8 %collective-permute-done.30 = bf16[2048,256]{1,0:T(8,128)(2,1)} collective-permute-done((bf16[2048,256]{1,0:T(8,128)(2,1)}, bf16[2048,256]{1,0:T(8,128)(2,1)}, u32[]{:S(2)}, u32[]{:S(2)}) %collective-permute-start.30) | collective-permute-done | bytes 1048608 | tf_op jit(solution)/shard_map/ppermute | solution.py:28
  182.7 9.0 %collective-permute-done.5 = bf16[256,1536]{1,0:T(8,128)(2,1)S(1)} collective-permute-done((bf16[256,1536]{1,0:T(8,128)(2,1)}, bf16[256,1536]{1,0:T(8,128)(2,1)S(1)}, u32[]{:S(2)}, u32[]{:S(2)}) %collective-permute-start.5) | collective-permute-done | bytes 786464 | tf_op jit(solution)/shard_map/ppermute | solution.py:31
  195.6 22.3 %collective-permute-done.24 = bf16[256,2048]{1,0:T(8,128)(2,1)S(1)} collective-permute-done((bf16[256,2048]{1,0:T(8,128)(2,1)}, bf16[256,2048]{1,0:T(8,128)(2,1)S(1)}, u32[]{:S(2)}, u32[]{:S(2)}) %collective-permute-start.24) | collective-permute-done | bytes 1048608 | tf_op jit(solution)/shard_map/ppermute | solution.py:21
  219.5 15.3 %collective-permute-done.7 = bf16[256,1536]{1,0:T(8,128)(2,1)S(1)} collective-permute-done((bf16[256,1536]{1,0:T(8,128)(2,1)S(1)}, bf16[256,1536]{1,0:T(8,128)(2,1)S(1)}, u32[]{:S(2)}, u32[]{:S(2)}) %collective-permute-start.7) | collective-permute-done | bytes 786464 | tf_op jit(solution)/shard_map/ppermute | solution.py:21
  237.1 5.6 %collective-permute-start.33 = (bf16[2048,256]{1,0:T(8,128)(2,1)}, bf16[2048,256]{1,0:T(8,128)(2,1)}, u32[]{:S(2)}, u32[]{:S(2)}) collective-permute-start(bf16[2048,256]{1,0:T(8,128)(2,1)} %constant_dynamic-slice_fusion.2), channel_id=1, source_target_pairs={{0,4},{4,8},{8,12},{1,5},{5,9},{9,13},{2,6},{6,10},{10,14},{3,7},{... | collective-permute-start | bytes 3145736 | tf_op jit(solution)/shard_map/ppermute | solution.py:29
  243.7 12.5 %collective-permute-done.31 = bf16[2048,256]{1,0:T(8,128)(2,1)S(1)} collective-permute-done((bf16[2048,256]{1,0:T(8,128)(2,1)}, bf16[2048,256]{1,0:T(8,128)(2,1)S(1)}, u32[]{:S(2)}, u32[]{:S(2)}) %collective-permute-start.31) | collective-permute-done | bytes 1048608 | tf_op jit(solution)/shard_map/ppermute | solution.py:21
  263.1 11.6 %collective-permute-done.9 = bf16[256,1536]{1,0:T(8,128)(2,1)S(1)} collective-permute-done((bf16[256,1536]{1,0:T(8,128)(2,1)S(1)}, bf16[256,1536]{1,0:T(8,128)(2,1)S(1)}, u32[]{:S(2)}, u32[]{:S(2)}) %collective-permute-start.9) | collective-permute-done | bytes 786464 | tf_op jit(solution)/shard_map/ppermute | solution.py:21
  276.2 9.6 %fusion.30 = (bf16[768,1536]{1,0:T(8,128)(2,1)S(1)}, f32[768,1536]{1,0:T(8,128)}) fusion(bf16[2048,1536]{1,0:T(8,128)(2,1)} %constant_dynamic-update-slice_fusion.25, bf16[768,2048]{1,0:T(8,128)(2,1)S(1)} %constant_dynamic-update-slice_fusion.32, f32[2048]{0:T(1024)S(1)} %convert_element_type.87, f32[768]{0:T(1024)S(1)} %add_rsqrt_fusion.2), kind=kOutput, calls=%fused_computation.110 | convolution fusion | flops 4839309312 | bytes 16526336 | tf_op jit(solution)/shard_map/dot_general | solution.py:62
  294.3 3.9 convolution_convert_fusion.1
  298.5 7.9 %collective-permute-done.32 = bf16[2048,256]{1,0:T(8,128)(2,1)} collective-permute-done((bf16[2048,256]{1,0:T(8,128)(2,1)}, bf16[2048,256]{1,0:T(8,128)(2,1)}, u32[]{:S(2)}, u32[]{:S(2)}) %collective-permute-start.32) | collective-permute-done | bytes 1048608 | tf_op jit(solution)/shard_map/ppermute | solution.py:31
  316.8 18.2 %collective-permute-done.34 = bf16[2048,256]{1,0:T(8,128)(2,1)S(1)} collective-permute-done((bf16[2048,256]{1,0:T(8,128)(2,1)S(1)}, bf16[2048,256]{1,0:T(8,128)(2,1)S(1)}, u32[]{:S(2)}, u32[]{:S(2)}) %collective-permute-start.34) | collective-permute-done | bytes 1048608 | tf_op jit(solution)/shard_map/ppermute | solution.py:21
  341.7 11.5 %collective-permute-done.21 = bf16[768,512]{1,0:T(8,128)(2,1)S(1)} collective-permute-done((bf16[768,512]{1,0:T(8,128)(2,1)S(1)}, bf16[768,512]{1,0:T(8,128)(2,1)S(1)}, u32[]{:S(2)}, u32[]{:S(2)}) %collective-permute-start.21) | collective-permute-done | bytes 786464 | tf_op jit(solution)/shard_map/ppermute | solution.py:21
  353.3 4.2 collective-permute-done.29
  358.5 18.3 %collective-permute-done.36 = bf16[2048,256]{1,0:T(8,128)(2,1)S(1)} collective-permute-done((bf16[2048,256]{1,0:T(8,128)(2,1)S(1)}, bf16[2048,256]{1,0:T(8,128)(2,1)S(1)}, u32[]{:S(2)}, u32[]{:S(2)}) %collective-permute-start.36) | collective-permute-done | bytes 1048608 | tf_op jit(solution)/shard_map/ppermute | solution.py:21
  379.1 20.8 %convolution_convert_fusion = bf16[768,2048]{1,0:T(8,128)(2,1)} fusion(bf16[2048,2048]{1,0:T(8,128)(2,1)} %constant_dynamic-update-slice_fusion, bf16[2048,2048]{1,0:T(8,128)(2,1)} %constant_dynamic-update-slice_fusion.7, bf16[768,2048]{1,0:T(8,128)(2,1)S(1)} %constant_dynamic-update-slice_fusion.14, f32[2048]{0:T(1024)S(1)} %convert_element_type.102, ...), kind=kOutput, calls=%fused_computation.11 | convolution fusion | flops 12897484800 | bytes 23079936 | tf_op jit(solution)/shard_map/dot_general | solution.py:62
  405.0 18.8 %collective-permute-done.38 = bf16[768,512]{1,0:T(8,128)(2,1)S(1)} collective-permute-done((bf16[768,512]{1,0:T(8,128)(2,1)S(1)}, bf16[768,512]{1,0:T(8,128)(2,1)S(1)}, u32[]{:S(2)}, u32[]{:S(2)}) %collective-permute-start.38) | collective-permute-done | bytes 786464 | tf_op jit(solution)/shard_map/ppermute | solution.py:21
  (166 shorter events, 110.9 us)
Async XLA Ops:
  0.0 134.4 %collective-permute-start = (bf16[768,512]{1,0:T(8,128)(2,1)}, bf16[768,512]{1,0:T(8,128)(2,1)}, u32[]{:S(2)}, u32[]{:S(2)}) collective-permute-start(bf16[768,512]{1,0:T(8,128)(2,1)} %param.11), channel_id=1, source_target_pairs={{0,1},{1,0},{2,3},{3,2},{4,5},{5,4},{6,7},{7,6},{8,9},{9,8},{10,11... | collective-permute-start | bytes 2359304 | tf_op jit(solution)/shard_map/ppermute | solution.py:66
  0.5 136.6 %collective-permute-start.1 = (bf16[768,512]{1,0:T(8,128)(2,1)}, bf16[768,512]{1,0:T(8,128)(2,1)}, u32[]{:S(2)}, u32[]{:S(2)}) collective-permute-start(bf16[768,512]{1,0:T(8,128)(2,1)} %param.11), channel_id=1, source_target_pairs={{0,2},{1,3},{2,0},{3,1},{4,6},{5,7},{6,4},{7,5},{8,10},{9,11},{10,... | collective-permute-start | bytes 2359304 | tf_op jit(solution)/shard_map/ppermute | solution.py:21
  4.7 27.9 %collective-permute-start.10 = (bf16[512,256]{1,0:T(8,128)(2,1)}, bf16[512,256]{1,0:T(8,128)(2,1)S(1)}, u32[]{:S(2)}, u32[]{:S(2)}) collective-permute-start(bf16[512,256]{1,0:T(8,128)(2,1)} %constant_dynamic-slice_fusion.6), channel_id=1, source_target_pairs={{0,8},{4,12},{8,0},{12,4},{1,9},{5,13},{9,1},{13,5},{2,10},{6,14},... | collective-permute-start | bytes 786440 | tf_op jit(solution)/shard_map/ppermute | solution.py:28
  7.2 35.3 %collective-permute-start.13 = (bf16[512,256]{1,0:T(8,128)(2,1)}, bf16[512,256]{1,0:T(8,128)(2,1)S(1)}, u32[]{:S(2)}, u32[]{:S(2)}) collective-permute-start(bf16[512,256]{1,0:T(8,128)(2,1)} %constant_dynamic-slice_fusion.6), channel_id=1, source_target_pairs={{0,4},{4,8},{8,12},{1,5},{5,9},{9,13},{2,6},{6,10},{10,14},{3,7},{... | collective-permute-start | bytes 786440 | tf_op jit(solution)/shard_map/ppermute | solution.py:29
  42.5 89.2 %collective-permute-start.3 = (bf16[256,1536]{1,0:T(8,128)(2,1)}, bf16[256,1536]{1,0:T(8,128)(2,1)}, u32[]{:S(2)}, u32[]{:S(2)}) collective-permute-start(bf16[256,1536]{1,0:T(8,128)(2,1)} %constant_dynamic-slice_fusion.7), channel_id=1, source_target_pairs={{0,8},{4,12},{8,0},{12,4},{1,9},{5,13},{9,1},{13,5},{2,10},{6,14},... | collective-permute-start | bytes 2359304 | tf_op jit(solution)/shard_map/ppermute | solution.py:28
  54.1 100.2 %collective-permute-start.23 = (bf16[256,2048]{1,0:T(8,128)(2,1)}, bf16[256,2048]{1,0:T(8,128)(2,1)}, u32[]{:S(2)}, u32[]{:S(2)}) collective-permute-start(bf16[256,2048]{1,0:T(8,128)(2,1)} %constant_dynamic-slice_fusion.3), channel_id=1, source_target_pairs={{0,8},{4,12},{8,0},{12,4},{1,9},{5,13},{9,1},{13,5},{2,10},{6,14},... | collective-permute-start | bytes 3145736 | tf_op jit(solution)/shard_map/ppermute | solution.py:28
  58.1 118.6 %collective-permute-start.30 = (bf16[2048,256]{1,0:T(8,128)(2,1)}, bf16[2048,256]{1,0:T(8,128)(2,1)}, u32[]{:S(2)}, u32[]{:S(2)}) collective-permute-start(bf16[2048,256]{1,0:T(8,128)(2,1)} %constant_dynamic-slice_fusion.2), channel_id=1, source_target_pairs={{0,8},{4,12},{8,0},{12,4},{1,9},{5,13},{9,1},{13,5},{2,10},{6,14},... | collective-permute-start | bytes 3145736 | tf_op jit(solution)/shard_map/ppermute | solution.py:28
  134.4 46.0 %collective-permute-start.4 = (bf16[256,1536]{1,0:T(8,128)(2,1)}, bf16[256,1536]{1,0:T(8,128)(2,1)S(1)}, u32[]{:S(2)}, u32[]{:S(2)}) collective-permute-start(bf16[256,1536]{1,0:T(8,128)(2,1)} %collective-permute-done.3), channel_id=1, source_target_pairs={{0,16},{16,0},{1,17},{17,1},{2,18},{18,2},{3,19},{19,3},{4,20},{20... | collective-permute-start | bytes 2359304 | tf_op jit(solution)/shard_map/ppermute | solution.py:21
  137.1 44.3 %collective-permute-start.6 = (bf16[256,1536]{1,0:T(8,128)(2,1)}, bf16[256,1536]{1,0:T(8,128)(2,1)S(1)}, u32[]{:S(2)}, u32[]{:S(2)}) collective-permute-start(bf16[256,1536]{1,0:T(8,128)(2,1)} %constant_dynamic-slice_fusion.7), channel_id=1, source_target_pairs={{0,4},{4,8},{8,12},{1,5},{5,9},{9,13},{2,6},{6,10},{10,14},{3,7},{... | collective-permute-start | bytes 2359304 | tf_op jit(solution)/shard_map/ppermute | solution.py:29
  140.9 50.8 %collective-permute-start.5 = (bf16[256,1536]{1,0:T(8,128)(2,1)}, bf16[256,1536]{1,0:T(8,128)(2,1)S(1)}, u32[]{:S(2)}, u32[]{:S(2)}) collective-permute-start(bf16[256,1536]{1,0:T(8,128)(2,1)} %collective-permute-done.3), channel_id=1, source_target_pairs={{4,0},{8,12},{5,1},{9,13},{6,2},{10,14},{7,3},{11,15},{20,16},{24,... | collective-permute-start | bytes 2359304 | tf_op jit(solution)/shard_map/ppermute | solution.py:31
  154.3 82.8 %collective-permute-start.8 = (bf16[256,1536]{1,0:T(8,128)(2,1)}, bf16[256,1536]{1,0:T(8,128)(2,1)S(1)}, u32[]{:S(2)}, u32[]{:S(2)}) collective-permute-start(bf16[256,1536]{1,0:T(8,128)(2,1)} %constant_dynamic-slice_fusion.7), channel_id=1, source_target_pairs={{4,0},{8,4},{12,8},{5,1},{9,5},{13,9},{6,2},{10,6},{14,10},{7,3},{... | collective-permute-start | bytes 2359304 | tf_op jit(solution)/shard_map/ppermute | solution.py:30
  176.7 81.2 %collective-permute-start.26 = (bf16[256,2048]{1,0:T(8,128)(2,1)}, bf16[256,2048]{1,0:T(8,128)(2,1)S(1)}, u32[]{:S(2)}, u32[]{:S(2)}) collective-permute-start(bf16[256,2048]{1,0:T(8,128)(2,1)} %constant_dynamic-slice_fusion.3), channel_id=1, source_target_pairs={{0,4},{4,8},{8,12},{1,5},{5,9},{9,13},{2,6},{6,10},{10,14},{3,7},{... | collective-permute-start | bytes 3145736 | tf_op jit(solution)/shard_map/ppermute | solution.py:29
  181.4 132.3 %collective-permute-start.28 = (bf16[256,2048]{1,0:T(8,128)(2,1)}, bf16[256,2048]{1,0:T(8,128)(2,1)}, u32[]{:S(2)}, u32[]{:S(2)}) collective-permute-start(bf16[256,2048]{1,0:T(8,128)(2,1)} %constant_dynamic-slice_fusion.3), channel_id=1, source_target_pairs={{4,0},{8,4},{12,8},{5,1},{9,5},{13,9},{6,2},{10,6},{14,10},{7,3},{... | collective-permute-start | bytes 3145736 | tf_op jit(solution)/shard_map/ppermute | solution.py:30
  191.7 26.2 %collective-permute-start.24 = (bf16[256,2048]{1,0:T(8,128)(2,1)}, bf16[256,2048]{1,0:T(8,128)(2,1)S(1)}, u32[]{:S(2)}, u32[]{:S(2)}) collective-permute-start(bf16[256,2048]{1,0:T(8,128)(2,1)} %collective-permute-done.23), channel_id=1, source_target_pairs={{0,16},{16,0},{1,17},{17,1},{2,18},{18,2},{3,19},{19,3},{4,20},{20... | collective-permute-start | bytes 3145736 | tf_op jit(solution)/shard_map/ppermute | solution.py:21
  193.3 41.5 %collective-permute-start.7 = (bf16[256,1536]{1,0:T(8,128)(2,1)S(1)}, bf16[256,1536]{1,0:T(8,128)(2,1)S(1)}, u32[]{:S(2)}, u32[]{:S(2)}) collective-permute-start(bf16[256,1536]{1,0:T(8,128)(2,1)S(1)} %get-tuple-element.10), channel_id=1, source_target_pairs={{0,16},{16,0},{1,17},{17,1},{2,18},{18,2},{3,19},{19,3},{4,20},{20... | collective-permute-start | bytes 2359304 | tf_op jit(solution)/shard_map/ppermute | solution.py:21
  218.0 38.3 %collective-permute-start.31 = (bf16[2048,256]{1,0:T(8,128)(2,1)}, bf16[2048,256]{1,0:T(8,128)(2,1)S(1)}, u32[]{:S(2)}, u32[]{:S(2)}) collective-permute-start(bf16[2048,256]{1,0:T(8,128)(2,1)} %collective-permute-done.30), channel_id=1, source_target_pairs={{0,16},{16,0},{1,17},{17,1},{2,18},{18,2},{3,19},{19,3},{4,20},{20... | collective-permute-start | bytes 3145736 | tf_op jit(solution)/shard_map/ppermute | solution.py:21
  237.1 61.4 %collective-permute-start.33 = (bf16[2048,256]{1,0:T(8,128)(2,1)}, bf16[2048,256]{1,0:T(8,128)(2,1)}, u32[]{:S(2)}, u32[]{:S(2)}) collective-permute-start(bf16[2048,256]{1,0:T(8,128)(2,1)} %constant_dynamic-slice_fusion.2), channel_id=1, source_target_pairs={{0,4},{4,8},{8,12},{1,5},{5,9},{9,13},{2,6},{6,10},{10,14},{3,7},{... | collective-permute-start | bytes 3145736 | tf_op jit(solution)/shard_map/ppermute | solution.py:29
  257.9 79.7 %collective-permute-start.35 = (bf16[2048,256]{1,0:T(8,128)(2,1)}, bf16[2048,256]{1,0:T(8,128)(2,1)}, u32[]{:S(2)}, u32[]{:S(2)}) collective-permute-start(bf16[2048,256]{1,0:T(8,128)(2,1)} %constant_dynamic-slice_fusion.2), channel_id=1, source_target_pairs={{4,0},{8,4},{12,8},{5,1},{9,5},{13,9},{6,2},{10,6},{14,10},{7,3},{... | collective-permute-start | bytes 3145736 | tf_op jit(solution)/shard_map/ppermute | solution.py:30
  260.0 46.4 %collective-permute-start.32 = (bf16[2048,256]{1,0:T(8,128)(2,1)}, bf16[2048,256]{1,0:T(8,128)(2,1)}, u32[]{:S(2)}, u32[]{:S(2)}) collective-permute-start(bf16[2048,256]{1,0:T(8,128)(2,1)} %collective-permute-done.30), channel_id=1, source_target_pairs={{4,0},{8,12},{5,1},{9,13},{6,2},{10,14},{7,3},{11,15},{20,16},{24,... | collective-permute-start | bytes 3145736 | tf_op jit(solution)/shard_map/ppermute | solution.py:31
  274.8 35.7 %collective-permute-start.27 = (bf16[256,2048]{1,0:T(8,128)(2,1)}, bf16[256,2048]{1,0:T(8,128)(2,1)}, u32[]{:S(2)}, u32[]{:S(2)}) collective-permute-start(bf16[256,2048]{1,0:T(8,128)(2,1)} %get-tuple-element.18), channel_id=1, source_target_pairs={{0,16},{16,0},{1,17},{17,1},{2,18},{18,2},{3,19},{19,3},{4,20},{20... | collective-permute-start | bytes 3145736 | tf_op jit(solution)/shard_map/ppermute | solution.py:21
  308.9 26.0 %collective-permute-start.34 = (bf16[2048,256]{1,0:T(8,128)(2,1)S(1)}, bf16[2048,256]{1,0:T(8,128)(2,1)S(1)}, u32[]{:S(2)}, u32[]{:S(2)}) collective-permute-start(bf16[2048,256]{1,0:T(8,128)(2,1)S(1)} %get-tuple-element.22), channel_id=1, source_target_pairs={{0,16},{16,0},{1,17},{17,1},{2,18},{18,2},{3,19},{19,3},{4,20},{20... | collective-permute-start | bytes 3145736 | tf_op jit(solution)/shard_map/ppermute | solution.py:21
  316.2 41.2 %collective-permute-start.29 = (bf16[256,2048]{1,0:T(8,128)(2,1)S(1)}, bf16[256,2048]{1,0:T(8,128)(2,1)S(1)}, u32[]{:S(2)}, u32[]{:S(2)}) collective-permute-start(bf16[256,2048]{1,0:T(8,128)(2,1)S(1)} %get-tuple-element.16), channel_id=1, source_target_pairs={{0,16},{16,0},{1,17},{17,1},{2,18},{18,2},{3,19},{19,3},{4,20},{20... | collective-permute-start | bytes 3145736 | tf_op jit(solution)/shard_map/ppermute | solution.py:21
  340.2 36.7 %collective-permute-start.36 = (bf16[2048,256]{1,0:T(8,128)(2,1)S(1)}, bf16[2048,256]{1,0:T(8,128)(2,1)S(1)}, u32[]{:S(2)}, u32[]{:S(2)}) collective-permute-start(bf16[2048,256]{1,0:T(8,128)(2,1)S(1)} %get-tuple-element.20), channel_id=1, source_target_pairs={{0,16},{16,0},{1,17},{17,1},{2,18},{18,2},{3,19},{19,3},{4,20},{20... | collective-permute-start | bytes 3145736 | tf_op jit(solution)/shard_map/ppermute | solution.py:21
  341.7 36.3 %collective-permute-start.20 = (bf16[768,512]{1,0:T(8,128)(2,1)S(1)}, bf16[768,512]{1,0:T(8,128)(2,1)S(1)}, u32[]{:S(2)}, u32[]{:S(2)}) collective-permute-start(bf16[768,512]{1,0:T(8,128)(2,1)S(1)} %get-tuple-element.6), channel_id=1, source_target_pairs={{0,1},{1,0},{2,3},{3,2},{4,5},{5,4},{6,7},{7,6},{8,9},{9,8},{10,11... | collective-permute-start | bytes 2359304 | tf_op jit(solution)/shard_map/ppermute | solution.py:66
  (32 other events, 373.1 us)
